TPU v7x, 32 devices: a whole 2x2x4 slice. The times are simulated.
32 devices in a mesh: sp: 8 (over z, x), tp: 4 (over y, core).
Axes of the slice: x: 2, y: 2, z: 4, core: 2. Of those that a mesh axis runs over, the one named last changes fastest.
Arguments:
- tokens: bfloat16 [2, 1536, 4096], P(None, 'sp', 'tp'), may hold values from -12 to 12
- query_weight: bfloat16 [4096, 2048], P(None, 'tp'), may hold values from -0.09375 to 0.09375
- key_weight: bfloat16 [4096, 2048], P(None, 'tp'), may hold values from -0.09375 to 0.09375
- value_weight: bfloat16 [4096, 2048], P(None, 'tp'), may hold values from -0.09375 to 0.09375
- gate_weight: bfloat16 [4096, 2048], P(None, 'tp'), may hold values from -0.09375 to 0.09375
- beta_weight: bfloat16 [4096, 16], P(None, 'tp'), may hold values from -0.09375 to 0.09375
- decay_weight: bfloat16 [4096, 16], P(None, 'tp'), may hold values from -0.09375 to 0.09375
- beta_bias: float32 [16], P('tp'), may hold values from -6 to -3
- rate_log: float32 [16], P('tp'), may hold values from -12 to -2.5
- out_gain: float32 [128], replicated, may hold values from 0.1 to 1.9
- new_query: bfloat16 [2, 16, 128], P(None, 'tp'), may hold values from -6 to 6
- new_key: bfloat16 [2, 16, 128], P(None, 'tp'), may hold values from -6 to 6
- new_value: bfloat16 [2, 16, 128], P(None, 'tp'), may hold values from -6 to 6
- new_beta: float32 [2, 16], P(None, 'tp'), may hold values from 0.1 to 0.9
- new_decay: float32 [2, 16], P(None, 'tp'), may hold values from 0.3 to 1
Outputs:
- mixed_out: bfloat16 [2, 1536, 2048], P(None, 'sp', 'tp')
- cache: bfloat16 [2, 16, 128, 128], P(None, 'tp', 'sp')
- first_out: float32 [2, 2048], P(None, 'tp')
All inputs are finite; a program needn't handle non-finite values.
Results may differ from a plain program's by a relative error of at most 0.0073.
Values may be sent and summed in bfloat16 or wider, within the bound.
A program may use at most 64 MiB of HBM per device.

v0:
```python
import jax
import jax.numpy as jnp
from jax import lax
from jax.sharding import PartitionSpec as P

BLOCK = 64
unit_floor = 1.0
norm_floor = 0.001
highest = lax.Precision.HIGHEST


def shifted(value, axis, steps):
    count = lax.axis_size(axis)
    first, last = (max(0, -steps), min(count, count - steps))
    return lax.ppermute(value, axis, [(source, source + steps) for source in range(first, last)])


def matmul(form, left, right):
    return jnp.einsum(form, left, right, precision=highest)


def unit_rows(values):
    return values * lax.rsqrt(jnp.sum(values * values, axis=-1, keepdims=True) + unit_floor)


def head_norm(values, out_gain):
    return (
        values
        * lax.rsqrt(jnp.mean(values * values, axis=-1, keepdims=True) + norm_floor)
        * out_gain
    )


def stored(values):
    return lax.optimization_barrier(values.astype(jnp.bfloat16)).astype(jnp.float32)


def unit_lower_inverse(lower_part):
    extent = lower_part.shape[-1]
    nilpotent = -lower_part
    inverse = jnp.eye(extent, dtype=jnp.float32) + nilpotent
    for _ in range(extent.bit_length() - 2):
        nilpotent = matmul("...ij,...jk->...ik", nilpotent, nilpotent)
        inverse = inverse + matmul("...ij,...jk->...ik", nilpotent, inverse)
    return inverse


def prepare(
    query_rows,
    key_rows,
    value_rows,
    beta_in,
    decay_in,
    beta_bias,
    rate_log,
    seq_count,
    length,
    head_count,
):
    extent = query_rows.shape[-1] // head_count
    blocks = length // BLOCK

    def by_head(values):
        shaped = values.reshape(seq_count, blocks, BLOCK, head_count, extent)
        return shaped.transpose(0, 3, 1, 2, 4).reshape(
            seq_count * head_count, blocks, BLOCK, extent
        )

    def by_scalar(values):
        shaped = values.reshape(seq_count, blocks, BLOCK, head_count)
        return shaped.transpose(0, 3, 1, 2).reshape(seq_count * head_count, blocks, BLOCK)

    queries = unit_rows(by_head(query_rows))
    key_unit = unit_rows(by_head(key_rows))
    values = by_head(value_rows)
    strength = by_scalar(jax.nn.sigmoid(beta_in + beta_bias))
    decays = by_scalar(-jnp.exp(rate_log) * jax.nn.softplus(decay_in))
    return (queries, key_unit, values, strength, decays)


def block_terms(queries, key_unit, values, strength, decays):
    extent = decays.shape[-1]
    cumulative = jnp.cumsum(decays, axis=-1)
    causal = jnp.tril(jnp.ones((extent, extent), bool))
    strict = jnp.tril(jnp.ones((extent, extent), bool), -1)
    spread = cumulative[..., :, None] - cumulative[..., None, :]
    weights = jnp.where(causal, jnp.exp(jnp.where(causal, spread, 0.0)), 0.0)
    key_beta = key_unit * strength[..., None]
    lower_part = jnp.where(strict, matmul("...td,...sd->...ts", key_beta, key_unit) * weights, 0.0)
    inverse = unit_lower_inverse(lower_part)
    update = matmul("...ts,...se->...te", inverse, values * strength[..., None])
    carry_w = matmul("...ts,...sd->...td", inverse, key_beta * jnp.exp(cumulative)[..., None])
    scores = matmul("...td,...sd->...ts", queries, key_unit) * weights
    query_decay = queries * jnp.exp(cumulative)[..., None]
    last_log = cumulative[..., -1]
    key_decay = key_unit * jnp.exp(last_log[..., None] - cumulative)[..., None]
    return (update, carry_w, query_decay, scores, key_decay, last_log)


def finish_read(recall, retrieve, query_unit, key_unit, new_value, new_beta, new_decay, out_gain):
    seq_count, head_count, extent = recall.shape
    intersect = jnp.sum(key_unit * query_unit, axis=-1)
    fresh_values = new_value.astype(jnp.float32) - new_decay[..., None] * retrieve
    read_heads = new_decay[..., None] * recall + (new_beta * intersect)[..., None] * fresh_values
    return head_norm(read_heads, out_gain).reshape(seq_count, head_count * extent)


def project_rows(shard_rows, weights):
    row_count = shard_rows.shape[-1]
    flat_rows = shard_rows.reshape(-1, row_count)
    return tuple(
        (jnp.dot(flat_rows, weight, preferred_element_type=jnp.float32) for weight in weights)
    )


def shards(
    tokens,
    query_weight,
    key_weight,
    value_weight,
    gate_weight,
    beta_weight,
    decay_weight,
    beta_bias,
    rate_log,
    out_gain,
    new_query,
    new_key,
    new_value,
    new_beta,
    new_decay,
):
    seq_count, span_len, _ = tokens.shape
    head_count = rate_log.shape[0]
    weights = (query_weight, key_weight, value_weight, gate_weight, beta_weight, decay_weight)
    totals = project_rows(lax.all_gather(tokens, "tp", axis=2, tiled=True), weights)
    query_rows = stored(totals[0])
    key_rows = stored(totals[1])
    value_rows = stored(totals[2])
    gate_rows = stored(totals[3])
    prepared = prepare(
        query_rows,
        key_rows,
        value_rows,
        totals[4],
        totals[5],
        beta_bias,
        rate_log,
        seq_count,
        span_len,
        head_count,
    )
    block_data = block_terms(*prepared)
    batch_size = block_data[0].shape[0]
    extent = block_data[0].shape[-1]
    identity = jnp.broadcast_to(jnp.eye(extent, dtype=jnp.float32), (batch_size, extent, extent))

    def advance(carried, inputs):
        state_now, reach_map = carried
        u_block, w_block, qg_block, score_block, kd_block, gl_block = inputs
        fresh_values = u_block - matmul("btd,bde->bte", w_block, state_now)
        block_out = matmul("btd,bde->bte", qg_block, state_now) + matmul(
            "bts,bse->bte", score_block, fresh_values
        )
        reach_rows = qg_block - matmul("bts,bsd->btd", score_block, w_block)
        factor = jnp.exp(gl_block)[:, None, None]
        transit = factor * identity - matmul("bsd,bse->bde", kd_block, w_block)
        state_next = state_now * factor + matmul("bsd,bse->bde", kd_block, fresh_values)
        map_next = matmul("bde,bef->bdf", transit, reach_map)
        return ((state_next, map_next), (block_out, matmul("btd,bde->bte", reach_rows, reach_map)))

    inputs = tuple((jnp.moveaxis(member, 1, 0) for member in block_data))
    start_state = jnp.zeros((batch_size, extent, extent), jnp.float32)
    (local_state, local_map), (local_out, reach_all) = lax.scan(
        advance, (start_state, identity), inputs
    )

    def turn(turn_index, incoming):
        outgoing = matmul("bde,bef->bdf", local_map, incoming) + local_state
        return shifted(outgoing, "sp", 1)

    incoming = lax.fori_loop(0, lax.axis_size("sp") - 1, turn, jnp.zeros_like(local_state))
    block_total = local_out + matmul("nbtd,bde->nbte", reach_all, incoming)
    blocks = span_len // BLOCK
    heads_out = block_total.reshape(blocks, seq_count, head_count, BLOCK, extent).transpose(
        1, 0, 3, 2, 4
    )
    heads_out = heads_out.reshape(seq_count, span_len, head_count, extent)
    gate_values = gate_rows.reshape(seq_count, span_len, head_count, extent)
    mixed_out = (head_norm(heads_out, out_gain) * jax.nn.silu(gate_values)).astype(jnp.bfloat16)
    mixed_out = mixed_out.reshape(seq_count, span_len, head_count * extent)
    final_state = matmul("bde,bef->bdf", local_map, incoming) + local_state
    final_cast = final_state.reshape(seq_count, head_count, extent, extent).astype(jnp.bfloat16)
    row_count = extent // lax.axis_size("sp")
    row_start = lax.axis_index("sp") * row_count
    query_unit = unit_rows(new_query.astype(jnp.float32))
    key_unit = unit_rows(new_key.astype(jnp.float32))
    is_last = lax.axis_index("sp") == lax.axis_size("sp") - 1
    own_term = jnp.where(is_last, final_cast.astype(jnp.float32), 0.0)
    cache_rows = lax.psum_scatter(
        own_term.astype(jnp.bfloat16), "sp", scatter_dimension=2, tiled=True
    )
    memory = lax.optimization_barrier(cache_rows).astype(jnp.float32)
    query_part = lax.dynamic_slice_in_dim(query_unit, row_start, row_count, 2)
    key_part = lax.dynamic_slice_in_dim(key_unit, row_start, row_count, 2)
    recall, retrieve = lax.psum(
        (matmul("shde,shd->she", memory, query_part), matmul("shde,shd->she", memory, key_part)),
        "sp",
    )
    first_out = finish_read(
        recall, retrieve, query_unit, key_unit, new_value, new_beta, new_decay, out_gain
    )
    return (mixed_out, cache_rows, first_out)


def solution(mesh):
    placed = (
        P(None, "sp", "tp"),
        P(None, "tp"),
        P(None, "tp"),
        P(None, "tp"),
        P(None, "tp"),
        P(None, "tp"),
        P(None, "tp"),
        P("tp"),
        P("tp"),
        P(),
        P(None, "tp", None),
        P(None, "tp", None),
        P(None, "tp", None),
        P(None, "tp"),
        P(None, "tp"),
    )
    return jax.shard_map(
        shards,
        mesh=mesh,
        in_specs=placed,
        out_specs=(P(None, "sp", "tp"), P(None, "tp", "sp", None), P(None, "tp")),
        check_vma=False,
    )
```

profile of v0, /device:TPU:0, one launch (start us, length us, event | category | flops | bytes accessed | tf_op | source)
XLA Modules:
  0.0 305.5 jit_solution(13586617555090404799)
XLA Ops:
  13.8 27.1 %all-gather.2.cloned.1.call-done = bf16[2,192,4096]{2,1,0:T(8,128)(2,1)} async-done(((bf16[2,192,1024]{2,1,0:T(8,128)(2,1)}), bf16[2,192,4096]{2,1,0:T(8,128)(2,1)}) %all-gather.2.cloned.1.call-update) | async-done | bytes 3145744 | tf_op jit(solution)/shard_map/all_gather | solution.py:136
  40.9 2.8 fusion.66
  44.7 5.8 %convolution_convert_fusion = bf16[384,512]{1,0:T(8,128)(2,1)} fusion(bf16[384,4096]{1,0:T(8,128)(2,1)} %bitcast.200, bf16[4096,512]{1,0:T(8,128)(2,1)} %param.23), kind=kOutput, calls=%fused_computation.59 | convolution fusion | flops 1610809344 | bytes 7733248 | tf_op jit(solution)/shard_map/dot_general | solution.py:112
  50.6 1.8 convolution_convert_fusion.1
  53.4 2.8 fusion.49
  56.3 4.9 %convolution_convert_fusion.3 = bf16[384,512]{1,0:T(8,128)(2,1)S(1)} fusion(bf16[384,4096]{1,0:T(8,128)(2,1)} %bitcast.202, bf16[4096,512]{1,0:T(8,128)(2,1)} %param.21), kind=kOutput, calls=%fused_computation.62 | convolution fusion | flops 1610809344 | bytes 7733248 | tf_op jit(solution)/shard_map/dot_general | solution.py:112
  62.2 4.9 %convolution_convert_fusion.2 = bf16[384,512]{1,0:T(8,128)(2,1)S(1)} fusion(bf16[384,4096]{1,0:T(8,128)(2,1)} %bitcast.203, bf16[4096,512]{1,0:T(8,128)(2,1)} %param.22), kind=kOutput, calls=%fused_computation.61 | convolution fusion | flops 1610809344 | bytes 7733248 | tf_op jit(solution)/shard_map/dot_general | solution.py:112
  67.6 1.2 multiply_bitcast_fusion
  69.0 1.4 fusion.41
  79.7 2.0 convolution_bitcast_fusion.4
  81.7 0.9 convolution_bitcast_fusion.3
  82.6 2.3 fusion.38
  85.0 23.5 %while.28 = (s32[]{:T(128)}, f32[8,128,128]{2,1,0:T(8,128)S(1)}, f32[8,128,128]{2,1,0:T(8,128)S(1)}, f32[3,8,64,128]{3,2,0,1:T(8,128)}, f32[3,8,64,128]{3,2,0,1:...) while((s32[]{:T(128)}, f32[8,128,128]{2,1,0:T(8,128)S(1)}, ...), condition=%wide.region_4.5_spmd.clone, body=%wide.region_3.4_spmd.clone.sunk | while | flops 806420480 | bytes 12392708 | solution.py:174
  85.6 1.5 convolution_subtract_fusion.6
  87.2 1.1 convolution_add_fusion.13
  88.7 1.3 fusion.170
  90.0 1.0 convolution_subtract_fusion.7
  91.7 1.1 fusion.169
  93.4 1.5 convolution_subtract_fusion.6
  95.0 1.1 convolution_add_fusion.13
  96.6 1.3 fusion.170
  97.9 1.0 convolution_subtract_fusion.7
  99.6 1.1 fusion.169
  101.3 1.5 convolution_subtract_fusion.6
  102.8 1.1 convolution_add_fusion.13
  104.4 1.3 fusion.170
  105.7 1.0 convolution_subtract_fusion.7
  107.4 1.1 fusion.169
  108.5 101.1 %while.27 = (s32[]{:T(128)}, f32[8,128,128]{2,1,0:T(8,128)S(1)}, f32[8,128,128]{2,1,0:T(8,128)S(1)}, f32[8,128,128]{2,1,0:T(8,128)S(1)}, s32[]{:T(128)}) while((s32[]{:T(128)}, f32[8,128,128]{2,1,0:T(8,128)S(1)}, f32[8,128,128]{2,1,0:T(8,128)S(1)}, f32[8,128,128]{2,1,0:T(8,128)S(1)}, s32[]{:T(128)}) %tuple.60), condition=%wide.region_6.7_spmd, body=%wide.region_5.6_spmd.sunk | while | flops 201457664 | bytes 4194405 | solution.py:182
  109.2 3.4 %collective-permute-start = (f32[8,128,128]{2,1,0:T(8,128)S(1)}, f32[8,128,128]{2,1,0:T(8,128)S(1)}, u32[]{:S(2)}, u32[]{:S(2)}) collective-permute-start(f32[8,128,128]{2,1,0:T(8,128)S(1)} %convolution_add_fusion.12), channel_id=1, source_target_pairs={{0,4},{4,8},{8,12},{12,16},{16,20},{20,24},{24,28},{1,5},{5,9},{9,... | collective-permute-start | bytes 1572872 | tf_op jit(solution)/shard_map/while/body/eval_jaxpr/ppermute | solution.py:15
  112.6 11.5 %collective-permute-done = f32[8,128,128]{2,1,0:T(8,128)S(1)} collective-permute-done((f32[8,128,128]{2,1,0:T(8,128)S(1)}, f32[8,128,128]{2,1,0:T(8,128)S(1)}, u32[]{:S(2)}, u32[]{:S(2)}) %collective-permute-start) | collective-permute-done | bytes 524320 | tf_op jit(solution)/shard_map/while/body/eval_jaxpr/ppermute | solution.py:15
  124.8 4.4 %collective-permute-start = (f32[8,128,128]{2,1,0:T(8,128)S(1)}, f32[8,128,128]{2,1,0:T(8,128)S(1)}, u32[]{:S(2)}, u32[]{:S(2)}) collective-permute-start(f32[8,128,128]{2,1,0:T(8,128)S(1)} %convolution_add_fusion.12), channel_id=1, source_target_pairs={{0,4},{4,8},{8,12},{12,16},{16,20},{20,24},{24,28},{1,5},{5,9},{9,... | collective-permute-start | bytes 1572872 | tf_op jit(solution)/shard_map/while/body/eval_jaxpr/ppermute | solution.py:15
  129.2 10.7 %collective-permute-done = f32[8,128,128]{2,1,0:T(8,128)S(1)} collective-permute-done((f32[8,128,128]{2,1,0:T(8,128)S(1)}, f32[8,128,128]{2,1,0:T(8,128)S(1)}, u32[]{:S(2)}, u32[]{:S(2)}) %collective-permute-start) | collective-permute-done | bytes 524320 | tf_op jit(solution)/shard_map/while/body/eval_jaxpr/ppermute | solution.py:15
  140.6 4.4 %collective-permute-start = (f32[8,128,128]{2,1,0:T(8,128)S(1)}, f32[8,128,128]{2,1,0:T(8,128)S(1)}, u32[]{:S(2)}, u32[]{:S(2)}) collective-permute-start(f32[8,128,128]{2,1,0:T(8,128)S(1)} %convolution_add_fusion.12), channel_id=1, source_target_pairs={{0,4},{4,8},{8,12},{12,16},{16,20},{20,24},{24,28},{1,5},{5,9},{9,... | collective-permute-start | bytes 1572872 | tf_op jit(solution)/shard_map/while/body/eval_jaxpr/ppermute | solution.py:15
  145.0 9.8 %collective-permute-done = f32[8,128,128]{2,1,0:T(8,128)S(1)} collective-permute-done((f32[8,128,128]{2,1,0:T(8,128)S(1)}, f32[8,128,128]{2,1,0:T(8,128)S(1)}, u32[]{:S(2)}, u32[]{:S(2)}) %collective-permute-start) | collective-permute-done | bytes 524320 | tf_op jit(solution)/shard_map/while/body/eval_jaxpr/ppermute | solution.py:15
  155.5 5.2 %collective-permute-start = (f32[8,128,128]{2,1,0:T(8,128)S(1)}, f32[8,128,128]{2,1,0:T(8,128)S(1)}, u32[]{:S(2)}, u32[]{:S(2)}) collective-permute-start(f32[8,128,128]{2,1,0:T(8,128)S(1)} %convolution_add_fusion.12), channel_id=1, source_target_pairs={{0,4},{4,8},{8,12},{12,16},{16,20},{20,24},{24,28},{1,5},{5,9},{9,... | collective-permute-start | bytes 1572872 | tf_op jit(solution)/shard_map/while/body/eval_jaxpr/ppermute | solution.py:15
  160.7 9.0 %collective-permute-done = f32[8,128,128]{2,1,0:T(8,128)S(1)} collective-permute-done((f32[8,128,128]{2,1,0:T(8,128)S(1)}, f32[8,128,128]{2,1,0:T(8,128)S(1)}, u32[]{:S(2)}, u32[]{:S(2)}) %collective-permute-start) | collective-permute-done | bytes 524320 | tf_op jit(solution)/shard_map/while/body/eval_jaxpr/ppermute | solution.py:15
  170.3 5.3 %collective-permute-start = (f32[8,128,128]{2,1,0:T(8,128)S(1)}, f32[8,128,128]{2,1,0:T(8,128)S(1)}, u32[]{:S(2)}, u32[]{:S(2)}) collective-permute-start(f32[8,128,128]{2,1,0:T(8,128)S(1)} %convolution_add_fusion.12), channel_id=1, source_target_pairs={{0,4},{4,8},{8,12},{12,16},{16,20},{20,24},{24,28},{1,5},{5,9},{9,... | collective-permute-start | bytes 1572872 | tf_op jit(solution)/shard_map/while/body/eval_jaxpr/ppermute | solution.py:15
  175.7 8.1 %collective-permute-done = f32[8,128,128]{2,1,0:T(8,128)S(1)} collective-permute-done((f32[8,128,128]{2,1,0:T(8,128)S(1)}, f32[8,128,128]{2,1,0:T(8,128)S(1)}, u32[]{:S(2)}, u32[]{:S(2)}) %collective-permute-start) | collective-permute-done | bytes 524320 | tf_op jit(solution)/shard_map/while/body/eval_jaxpr/ppermute | solution.py:15
  184.4 5.3 %collective-permute-start = (f32[8,128,128]{2,1,0:T(8,128)S(1)}, f32[8,128,128]{2,1,0:T(8,128)S(1)}, u32[]{:S(2)}, u32[]{:S(2)}) collective-permute-start(f32[8,128,128]{2,1,0:T(8,128)S(1)} %convolution_add_fusion.12), channel_id=1, source_target_pairs={{0,4},{4,8},{8,12},{12,16},{16,20},{20,24},{24,28},{1,5},{5,9},{9,... | collective-permute-start | bytes 1572872 | tf_op jit(solution)/shard_map/while/body/eval_jaxpr/ppermute | solution.py:15
  189.8 7.3 %collective-permute-done = f32[8,128,128]{2,1,0:T(8,128)S(1)} collective-permute-done((f32[8,128,128]{2,1,0:T(8,128)S(1)}, f32[8,128,128]{2,1,0:T(8,128)S(1)}, u32[]{:S(2)}, u32[]{:S(2)}) %collective-permute-start) | collective-permute-done | bytes 524320 | tf_op jit(solution)/shard_map/while/body/eval_jaxpr/ppermute | solution.py:15
  197.7 5.3 %collective-permute-start = (f32[8,128,128]{2,1,0:T(8,128)S(1)}, f32[8,128,128]{2,1,0:T(8,128)S(1)}, u32[]{:S(2)}, u32[]{:S(2)}) collective-permute-start(f32[8,128,128]{2,1,0:T(8,128)S(1)} %convolution_add_fusion.12), channel_id=1, source_target_pairs={{0,4},{4,8},{8,12},{12,16},{16,20},{20,24},{24,28},{1,5},{5,9},{9,... | collective-permute-start | bytes 1572872 | tf_op jit(solution)/shard_map/while/body/eval_jaxpr/ppermute | solution.py:15
  203.0 6.6 %collective-permute-done = f32[8,128,128]{2,1,0:T(8,128)S(1)} collective-permute-done((f32[8,128,128]{2,1,0:T(8,128)S(1)}, f32[8,128,128]{2,1,0:T(8,128)S(1)}, u32[]{:S(2)}, u32[]{:S(2)}) %collective-permute-start) | collective-permute-done | bytes 524320 | tf_op jit(solution)/shard_map/while/body/eval_jaxpr/ppermute | solution.py:15
  209.6 1.3 fusion.45
  211.0 1.9 fusion.39
  215.1 1.0 fusion.59
  216.2 60.0 %reduce-scatter.2.cloned.1.call-done = bf16[2,4,16,128]{3,2,1,0:T(8,128)(2,1)} async-done(((bf16[2,4,128,128]{3,2,1,0:T(8,128)(2,1)}), bf16[2,4,16,128]{3,2,1,0:T(8,128)(2,1)}) %reduce-scatter.2.cloned.1.call-update) | async-done | bytes 32784 | tf_op jit(solution)/shard_map/reduce_scatter | solution.py:200
  278.0 19.8 %all-reduce = (f32[2,4,128]{2,1,0:T(4,128)S(1)}, f32[2,4,128]{2,1,0:T(4,128)S(1)}) all-reduce(f32[2,4,128]{2,1,0:T(4,128)S(1)} %bitcast.225, f32[2,4,128]{2,1,0:T(4,128)S(1)} %bitcast.226), channel_id=1, replica_groups=mesh['sp'=8,'tp'=4] {'sp'}, use_global_device_ids=true, to_apply=%region_13.14 | all-reduce | flops 2048 | bytes 16384 | tf_op jit(solution)/shard_map/psum | solution.py:206
  (121 shorter events, 33.7 us)
Async XLA Ops:
  7.2 33.7 %copy-start = (bf16[4096,4]{0,1:T(4,128)(2,1)S(1)}, bf16[4096,4]{0,1:T(4,128)(2,1)}, u32[]{:S(2)}) copy-start(bf16[4096,4]{0,1:T(4,128)(2,1)} %param.25) | copy-start | bytes 98308
  7.2 33.7 %all-gather.2.cloned.1.call-start = ((), (), s32[]{:S(2)}) async-start(), calls=%async_computation.1 | async-start | bytes 3932160 | tf_op jit(solution)/shard_map/all_gather | solution.py:136
  7.9 268.2 %reduce-scatter.2.cloned.1.call-start = ((), (), s32[]{:S(2)}) async-start(), calls=%async_computation.2 | async-start | bytes 294912 | tf_op jit(solution)/shard_map/reduce_scatter | solution.py:200
  44.6 5.9 %copy-start.1 = (bf16[2,192,4096]{2,1,0:T(8,128)(2,1)S(1)}, bf16[2,192,4096]{2,1,0:T(8,128)(2,1)}, u32[]{:S(2)}) copy-start(bf16[2,192,4096]{2,1,0:T(8,128)(2,1)} %all-gather.2.cloned.1.call-done) | copy-start | bytes 9437188
  44.7 5.9 %copy-start.13 = (bf16[4096,512]{1,0:T(8,128)(2,1)S(1)}, bf16[4096,512]{1,0:T(8,128)(2,1)}, u32[]{:S(2)}) copy-start(bf16[4096,512]{1,0:T(8,128)(2,1)} %param.20) | copy-start | bytes 12582916
  52.4 1.0 copy-start.5
  52.4 1.0 copy-start.11
  67.5 1.5 copy-start.6
  85.0 3.3 %copy-start.2 = (f32[3,8,64,64]{3,2,0,1:T(8,128)S(1)}, f32[3,8,64,64]{3,2,0,1:T(8,128)}, u32[]{:S(2)}) copy-start(f32[3,8,64,64]{3,2,0,1:T(8,128)} %get-tuple-element.397) | copy-start | bytes 1179652 | tf_op jit(solution)/shard_map/while
  92.8 3.3 %copy-start.2 = (f32[3,8,64,64]{3,2,0,1:T(8,128)S(1)}, f32[3,8,64,64]{3,2,0,1:T(8,128)}, u32[]{:S(2)}) copy-start(f32[3,8,64,64]{3,2,0,1:T(8,128)} %get-tuple-element.397) | copy-start | bytes 1179652 | tf_op jit(solution)/shard_map/while
  100.7 3.3 %copy-start.2 = (f32[3,8,64,64]{3,2,0,1:T(8,128)S(1)}, f32[3,8,64,64]{3,2,0,1:T(8,128)}, u32[]{:S(2)}) copy-start(f32[3,8,64,64]{3,2,0,1:T(8,128)} %get-tuple-element.397) | copy-start | bytes 1179652 | tf_op jit(solution)/shard_map/while
  108.5 102.5 %copy-start.3 = (f32[3,8,64,128]{3,2,0,1:T(8,128)S(1)}, f32[3,8,64,128]{3,2,0,1:T(8,128)}, u32[]{:S(2)}) copy-start(f32[3,8,64,128]{3,2,0,1:T(8,128)} %get-tuple-element.90) | copy-start | bytes 2359300
  109.2 14.9 %collective-permute-start = (f32[8,128,128]{2,1,0:T(8,128)S(1)}, f32[8,128,128]{2,1,0:T(8,128)S(1)}, u32[]{:S(2)}, u32[]{:S(2)}) collective-permute-start(f32[8,128,128]{2,1,0:T(8,128)S(1)} %convolution_add_fusion.12), channel_id=1, source_target_pairs={{0,4},{4,8},{8,12},{12,16},{16,20},{20,24},{24,28},{1,5},{5,9},{9,... | collective-permute-start | bytes 1572872 | tf_op jit(solution)/shard_map/while/body/eval_jaxpr/ppermute | solution.py:15
  124.8 15.1 %collective-permute-start = (f32[8,128,128]{2,1,0:T(8,128)S(1)}, f32[8,128,128]{2,1,0:T(8,128)S(1)}, u32[]{:S(2)}, u32[]{:S(2)}) collective-permute-start(f32[8,128,128]{2,1,0:T(8,128)S(1)} %convolution_add_fusion.12), channel_id=1, source_target_pairs={{0,4},{4,8},{8,12},{12,16},{16,20},{20,24},{24,28},{1,5},{5,9},{9,... | collective-permute-start | bytes 1572872 | tf_op jit(solution)/shard_map/while/body/eval_jaxpr/ppermute | solution.py:15
  140.6 14.2 %collective-permute-start = (f32[8,128,128]{2,1,0:T(8,128)S(1)}, f32[8,128,128]{2,1,0:T(8,128)S(1)}, u32[]{:S(2)}, u32[]{:S(2)}) collective-permute-start(f32[8,128,128]{2,1,0:T(8,128)S(1)} %convolution_add_fusion.12), channel_id=1, source_target_pairs={{0,4},{4,8},{8,12},{12,16},{16,20},{20,24},{24,28},{1,5},{5,9},{9,... | collective-permute-start | bytes 1572872 | tf_op jit(solution)/shard_map/while/body/eval_jaxpr/ppermute | solution.py:15
  155.5 14.2 %collective-permute-start = (f32[8,128,128]{2,1,0:T(8,128)S(1)}, f32[8,128,128]{2,1,0:T(8,128)S(1)}, u32[]{:S(2)}, u32[]{:S(2)}) collective-permute-start(f32[8,128,128]{2,1,0:T(8,128)S(1)} %convolution_add_fusion.12), channel_id=1, source_target_pairs={{0,4},{4,8},{8,12},{12,16},{16,20},{20,24},{24,28},{1,5},{5,9},{9,... | collective-permute-start | bytes 1572872 | tf_op jit(solution)/shard_map/while/body/eval_jaxpr/ppermute | solution.py:15
  170.3 13.4 %collective-permute-start = (f32[8,128,128]{2,1,0:T(8,128)S(1)}, f32[8,128,128]{2,1,0:T(8,128)S(1)}, u32[]{:S(2)}, u32[]{:S(2)}) collective-permute-start(f32[8,128,128]{2,1,0:T(8,128)S(1)} %convolution_add_fusion.12), channel_id=1, source_target_pairs={{0,4},{4,8},{8,12},{12,16},{16,20},{20,24},{24,28},{1,5},{5,9},{9,... | collective-permute-start | bytes 1572872 | tf_op jit(solution)/shard_map/while/body/eval_jaxpr/ppermute | solution.py:15
  184.4 12.6 %collective-permute-start = (f32[8,128,128]{2,1,0:T(8,128)S(1)}, f32[8,128,128]{2,1,0:T(8,128)S(1)}, u32[]{:S(2)}, u32[]{:S(2)}) collective-permute-start(f32[8,128,128]{2,1,0:T(8,128)S(1)} %convolution_add_fusion.12), channel_id=1, source_target_pairs={{0,4},{4,8},{8,12},{12,16},{16,20},{20,24},{24,28},{1,5},{5,9},{9,... | collective-permute-start | bytes 1572872 | tf_op jit(solution)/shard_map/while/body/eval_jaxpr/ppermute | solution.py:15
  197.7 12.0 %collective-permute-start = (f32[8,128,128]{2,1,0:T(8,128)S(1)}, f32[8,128,128]{2,1,0:T(8,128)S(1)}, u32[]{:S(2)}, u32[]{:S(2)}) collective-permute-start(f32[8,128,128]{2,1,0:T(8,128)S(1)} %convolution_add_fusion.12), channel_id=1, source_target_pairs={{0,4},{4,8},{8,12},{12,16},{16,20},{20,24},{24,28},{1,5},{5,9},{9,... | collective-permute-start | bytes 1572872 | tf_op jit(solution)/shard_map/while/body/eval_jaxpr/ppermute | solution.py:15
  213.3 1.9 copy-start.4
  213.8 62.4 %copy-start.9 = (f32[2,4,16]{2,1,0:T(4,128)S(1)}, f32[2,4,16]{2,1,0:T(4,128)}, u32[]{:S(2)}) copy-start(f32[2,4,16]{2,1,0:T(4,128)} %get-tuple-element.259) | copy-start | bytes 1540
  213.8 63.3 %copy-start.8 = (f32[2,4,16]{2,1,0:T(4,128)S(1)}, f32[2,4,16]{2,1,0:T(4,128)}, u32[]{:S(2)}) copy-start(f32[2,4,16]{2,1,0:T(4,128)} %get-tuple-element.260) | copy-start | bytes 1540
  213.8 83.9 %copy-start.7 = (bf16[2,4,128]{2,1,0:T(4,128)(2,1)S(1)}, bf16[2,4,128]{2,1,0:T(4,128)(2,1)}, u32[]{:S(2)}) copy-start(bf16[2,4,128]{2,1,0:T(4,128)(2,1)} %param.31) | copy-start | bytes 6148
  213.8 83.9 %copy-start.10 = (f32[2,4]{1,0:T(2,128)S(1)}, f32[2,4]{1,0:T(2,128)}, u32[]{:S(2)}) copy-start(f32[2,4]{1,0:T(2,128)} %param.33) | copy-start | bytes 100
  213.8 84.1 %copy-start.12 = (f32[128]{0:T(128)S(1)}, f32[128]{0:T(128)}, u32[]{:S(2)}) copy-start(f32[128]{0:T(128)} %param.28) | copy-start | bytes 1540
Sparse Core Ops, SparseCore 0:
  9.5 31.2 all-gather.1
  211.1 64.9 reduce-scatter.1
where the time goes:
time: 306 us; the launch traced here: 305 us
  waiting for transfers between devices  151 us (49%)
  matrix products  71.6 us (23%)
  starting transfers between devices  33.5 us (11%)
  blocking collectives  19.8 us (6%)
  between operations  14.5 us (5%)
  other arithmetic  9.26 us (3%)
  local copies, waits for them, and re-layouts  5.57 us (2%)
    ppermute x7, waiting for transfers between devices, shifted(): lax.ppermute(value, axis, [(source, source + steps) for source in range(f...  63 us
    reduce_scatter x1, waiting for transfers between devices, shards(): lax.psum_scatter(own_term.astype(jnp.bfloat16), 'sp', scatter_dimension=2...  60 us
    dot_general x49, matrix products, matmul(): return jnp.einsum(form, left, right, precision=highest)  48.5 us
    ppermute x7, starting transfers between devices, shifted(): lax.ppermute(value, axis, [(source, source + steps) for source in range(f...  33.4 us
    all_gather x1, waiting for transfers between devices, shards(): lax.all_gather(tokens, 'tp', axis=2, tiled=True)  27.1 us
    dot_general x6, matrix products, project_rows(): jnp.dot(flat_rows, weight, preferred_element_type=jnp.float32)  23.1 us
    psum x1, blocking collectives, shards(): lax.psum((matmul('shde,shd->she', memory, query_part), matmul('shde,shd->...  19.8 us
  transfers between devices with their start and end apart: 9, of which 9 were waited for; matrix products, arithmetic and copies ran while one was open for 4% of the time, Pallas kernels for 0%

commit v1 on v0

--- a/solution.py
+++ b/solution.py
@@ -1,3 +1,4 @@
+import functools
 import jax
 import jax.numpy as jnp
 from jax import lax
@@ -7,6 +8,25 @@
 unit_floor = 1.0
 norm_floor = 0.001
 highest = lax.Precision.HIGHEST
+
+
+def cubes_report(w_in, pos_dim):
+    nodes = jax.lax.axis_size("tp")
+    copies = [w_in]
+    for pp in range(1, nodes):
+        copies.append(
+            jax.lax.ppermute(
+                copies[pp - 1], axis_name="tp", perm=[(no, (no - 1) % nodes) for no in range(nodes)]
+            )
+        )
+    return jnp.roll(
+        jnp.concatenate(copies, axis=pos_dim),
+        jax.lax.axis_index("tp") * w_in.shape[pos_dim],
+        axis=pos_dim,
+    )
+
+
+_put_loops = functools.partial(cubes_report, pos_dim=2)
 
 
 def shifted(value, axis, steps):
@@ -133,7 +153,7 @@
     seq_count, span_len, _ = tokens.shape
     head_count = rate_log.shape[0]
     weights = (query_weight, key_weight, value_weight, gate_weight, beta_weight, decay_weight)
-    totals = project_rows(lax.all_gather(tokens, "tp", axis=2, tiled=True), weights)
+    totals = project_rows(_put_loops(tokens), weights)
     query_rows = stored(totals[0])
     key_rows = stored(totals[1])
     value_rows = stored(totals[2])

time: 306 us -> 320 us (1.046)
  starting transfers between devices: 33.5 us -> 39.7 us
  matrix products: 71.6 us -> 75.5 us
  local copies, waits for them, and re-layouts: 5.57 us -> 9.2 us
    all_gather x1 -> x0, waiting for transfers between devices: 27.1 us -> none  [shards(): lax.all_gather(tokens, 'tp', axis=2, tiled=True)]
    ppermute x0 -> x3, waiting for transfers between devices: none -> 21.7 us  [cubes_report(): jax.lax.ppermute(copies[pp - 1], axis_name='tp', perm=[(no, (no - 1) % no...]
    ppermute x0 -> x3, starting transfers between devices: none -> 6.19 us  [cubes_report(): jax.lax.ppermute(copies[pp - 1], axis_name='tp', perm=[(no, (no - 1) % no...]
    dot_general x49, matrix products: 48.5 us -> 54.2 us  [matmul(): return jnp.einsum(form, left, right, precision=highest)]
    reduce_scatter x1, waiting for transfers between devices: 60 us -> 63.4 us  [shards(): lax.psum_scatter(own_term.astype(jnp.bfloat16), 'sp', scatter_dimension=2...]
    unnamed x27 -> x38, local copies, waits for them, and re-layouts: 0.69 us -> 3.92 us
  transfers between devices with their start and end apart: 9 -> 11, of which waited for: 9 -> 11; matrix products, arithmetic and copies ran while one was open for 4% -> 4% of each run, Pallas kernels for 0% -> 0%
where the time goes in v1:
time: 320 us; the launch traced here: 319 us
  waiting for transfers between devices  151 us (47%)
  matrix products  75.5 us (24%)
  starting transfers between devices  39.7 us (12%)
  blocking collectives  19.7 us (6%)
  between operations  14.6 us (5%)
  other arithmetic  9.24 us (3%)
  local copies, waits for them, and re-layouts  9.2 us (3%)
    ppermute x7, waiting for transfers between devices, shifted(): lax.ppermute(value, axis, [(source, source + steps) for source in range(f...  66 us
    reduce_scatter x1, waiting for transfers between devices, shards(): lax.psum_scatter(own_term.astype(jnp.bfloat16), 'sp', scatter_dimension=2...  63.4 us
    dot_general x49, matrix products, matmul(): return jnp.einsum(form, left, right, precision=highest)  54.2 us
    ppermute x7, starting transfers between devices, shifted(): lax.ppermute(value, axis, [(source, source + steps) for source in range(f...  33.5 us
    ppermute x3, waiting for transfers between devices, cubes_report(): jax.lax.ppermute(copies[pp - 1], axis_name='tp', perm=[(no, (no - 1) % no...  21.7 us
    dot_general x6, matrix products, project_rows(): jnp.dot(flat_rows, weight, preferred_element_type=jnp.float32)  21.2 us
    psum x1, blocking collectives, shards(): lax.psum((matmul('shde,shd->she', memory, query_part), matmul('shde,shd->...  19.7 us
  transfers between devices with their start and end apart: 11, of which 11 were waited for; matrix products, arithmetic and copies ran while one was open for 4% of the time, Pallas kernels for 0%

profile of v1, /device:TPU:0, one launch (start us, length us, event | category | flops | bytes accessed | tf_op | source)
XLA Modules:
  0.0 319.4 jit_solution(11661704949225231169)
XLA Ops:
  7.2 2.5 collective-permute-start.1
  11.3 8.3 %collective-permute-done.1 = bf16[2,192,1024]{2,1,0:T(8,128)(2,1)S(1)} collective-permute-done((bf16[2,192,1024]{2,1,0:T(8,128)(2,1)}, bf16[2,192,1024]{2,1,0:T(8,128)(2,1)S(1)}, u32[]{:S(2)}, u32[]{:S(2)}) %collective-permute-start.1) | collective-permute-done | bytes 786464 | tf_op jit(solution)/shard_map/ppermute | solution.py:18
  19.5 1.8 collective-permute-start.2
  25.4 5.4 %collective-permute-done.2 = bf16[2,192,1024]{2,1,0:T(8,128)(2,1)S(1)} collective-permute-done((bf16[2,192,1024]{2,1,0:T(8,128)(2,1)S(1)}, bf16[2,192,1024]{2,1,0:T(8,128)(2,1)S(1)}, u32[]{:S(2)}, u32[]{:S(2)}) %collective-permute-start.2) | collective-permute-done | bytes 786464 | tf_op jit(solution)/shard_map/ppermute | solution.py:18
  30.9 1.9 collective-permute-start.3
  34.2 8.0 %collective-permute-done.3 = bf16[2,192,1024]{2,1,0:T(8,128)(2,1)S(1)} collective-permute-done((bf16[2,192,1024]{2,1,0:T(8,128)(2,1)S(1)}, bf16[2,192,1024]{2,1,0:T(8,128)(2,1)S(1)}, u32[]{:S(2)}, u32[]{:S(2)}) %collective-permute-start.3) | collective-permute-done | bytes 786464 | tf_op jit(solution)/shard_map/ppermute | solution.py:18
  43.0 1.7 copy-done.1
  46.6 5.8 %convolution_convert_fusion = bf16[384,512]{1,0:T(8,128)(2,1)} fusion(bf16[384,4096]{1,0:T(8,128)(2,1)} %bitcast.200, bf16[4096,512]{1,0:T(8,128)(2,1)} %param.23), kind=kOutput, calls=%fused_computation.59 | convolution fusion | flops 1610809344 | bytes 7733248 | tf_op jit(solution)/shard_map/dot_general | solution.py:132
  52.5 1.8 convolution_convert_fusion.1
  55.3 2.8 fusion.49
  58.2 4.9 %convolution_convert_fusion.3 = bf16[384,512]{1,0:T(8,128)(2,1)S(1)} fusion(bf16[384,4096]{1,0:T(8,128)(2,1)} %bitcast.202, bf16[4096,512]{1,0:T(8,128)(2,1)} %param.21), kind=kOutput, calls=%fused_computation.62 | convolution fusion | flops 1610809344 | bytes 7733248 | tf_op jit(solution)/shard_map/dot_general | solution.py:132
  64.1 4.9 %convolution_convert_fusion.2 = bf16[384,512]{1,0:T(8,128)(2,1)S(1)} fusion(bf16[384,4096]{1,0:T(8,128)(2,1)} %bitcast.203, bf16[4096,512]{1,0:T(8,128)(2,1)} %param.22), kind=kOutput, calls=%fused_computation.61 | convolution fusion | flops 1610809344 | bytes 7733248 | tf_op jit(solution)/shard_map/dot_general | solution.py:132
  69.5 1.2 multiply_bitcast_fusion
  70.9 1.4 fusion.41
  81.6 2.0 convolution_bitcast_fusion.4
  84.5 2.3 fusion.38
  86.9 29.2 %while.28 = (s32[]{:T(128)}, f32[8,128,128]{2,1,0:T(8,128)S(1)}, f32[8,128,128]{2,1,0:T(8,128)S(1)}, f32[3,8,64,128]{3,2,0,1:T(8,128)}, f32[3,8,64,128]{3,2,0,1:...) while((s32[]{:T(128)}, f32[8,128,128]{2,1,0:T(8,128)S(1)}, ...), condition=%wide.region_4.5_spmd.clone, body=%wide.region_3.4_spmd.clone.sunk | while | flops 806420480 | bytes 10819816 | solution.py:194
  87.5 1.5 convolution_subtract_fusion.6
  90.2 1.3 convolution_subtract_fusion.8
  91.6 1.3 fusion.170
  94.6 2.1 fusion.169
  97.2 1.5 convolution_subtract_fusion.6
  99.9 1.3 convolution_subtract_fusion.8
  101.3 1.3 fusion.170
  104.3 2.1 fusion.169
  106.9 1.5 convolution_subtract_fusion.6
  109.6 1.3 convolution_subtract_fusion.8
  111.0 1.3 fusion.170
  114.0 2.0 fusion.169
  116.1 104.1 %while.27 = (s32[]{:T(128)}, f32[8,128,128]{2,1,0:T(8,128)S(1)}, f32[8,128,128]{2,1,0:T(8,128)S(1)}, f32[8,128,128]{2,1,0:T(8,128)S(1)}, s32[]{:T(128)}) while((s32[]{:T(128)}, f32[8,128,128]{2,1,0:T(8,128)S(1)}, f32[8,128,128]{2,1,0:T(8,128)S(1)}, f32[8,128,128]{2,1,0:T(8,128)S(1)}, s32[]{:T(128)}) %tuple.60), condition=%wide.region_6.7_spmd, body=%wide.region_5.6_spmd.sunk | while | flops 201457664 | bytes 4194405 | solution.py:202
  116.8 3.4 %collective-permute-start = (f32[8,128,128]{2,1,0:T(8,128)S(1)}, f32[8,128,128]{2,1,0:T(8,128)S(1)}, u32[]{:S(2)}, u32[]{:S(2)}) collective-permute-start(f32[8,128,128]{2,1,0:T(8,128)S(1)} %convolution_add_fusion.12), channel_id=1, source_target_pairs={{0,4},{4,8},{8,12},{12,16},{16,20},{20,24},{24,28},{1,5},{5,9},{9,... | collective-permute-start | bytes 1572872 | tf_op jit(solution)/shard_map/while/body/eval_jaxpr/ppermute | solution.py:35
  120.2 12.0 %collective-permute-done = f32[8,128,128]{2,1,0:T(8,128)S(1)} collective-permute-done((f32[8,128,128]{2,1,0:T(8,128)S(1)}, f32[8,128,128]{2,1,0:T(8,128)S(1)}, u32[]{:S(2)}, u32[]{:S(2)}) %collective-permute-start) | collective-permute-done | bytes 524320 | tf_op jit(solution)/shard_map/while/body/eval_jaxpr/ppermute | solution.py:35
  132.9 4.4 %collective-permute-start = (f32[8,128,128]{2,1,0:T(8,128)S(1)}, f32[8,128,128]{2,1,0:T(8,128)S(1)}, u32[]{:S(2)}, u32[]{:S(2)}) collective-permute-start(f32[8,128,128]{2,1,0:T(8,128)S(1)} %convolution_add_fusion.12), channel_id=1, source_target_pairs={{0,4},{4,8},{8,12},{12,16},{16,20},{20,24},{24,28},{1,5},{5,9},{9,... | collective-permute-start | bytes 1572872 | tf_op jit(solution)/shard_map/while/body/eval_jaxpr/ppermute | solution.py:35
  137.3 11.1 %collective-permute-done = f32[8,128,128]{2,1,0:T(8,128)S(1)} collective-permute-done((f32[8,128,128]{2,1,0:T(8,128)S(1)}, f32[8,128,128]{2,1,0:T(8,128)S(1)}, u32[]{:S(2)}, u32[]{:S(2)}) %collective-permute-start) | collective-permute-done | bytes 524320 | tf_op jit(solution)/shard_map/while/body/eval_jaxpr/ppermute | solution.py:35
  149.1 4.4 %collective-permute-start = (f32[8,128,128]{2,1,0:T(8,128)S(1)}, f32[8,128,128]{2,1,0:T(8,128)S(1)}, u32[]{:S(2)}, u32[]{:S(2)}) collective-permute-start(f32[8,128,128]{2,1,0:T(8,128)S(1)} %convolution_add_fusion.12), channel_id=1, source_target_pairs={{0,4},{4,8},{8,12},{12,16},{16,20},{20,24},{24,28},{1,5},{5,9},{9,... | collective-permute-start | bytes 1572872 | tf_op jit(solution)/shard_map/while/body/eval_jaxpr/ppermute | solution.py:35
  153.5 10.3 %collective-permute-done = f32[8,128,128]{2,1,0:T(8,128)S(1)} collective-permute-done((f32[8,128,128]{2,1,0:T(8,128)S(1)}, f32[8,128,128]{2,1,0:T(8,128)S(1)}, u32[]{:S(2)}, u32[]{:S(2)}) %collective-permute-start) | collective-permute-done | bytes 524320 | tf_op jit(solution)/shard_map/while/body/eval_jaxpr/ppermute | solution.py:35
  164.5 5.3 %collective-permute-start = (f32[8,128,128]{2,1,0:T(8,128)S(1)}, f32[8,128,128]{2,1,0:T(8,128)S(1)}, u32[]{:S(2)}, u32[]{:S(2)}) collective-permute-start(f32[8,128,128]{2,1,0:T(8,128)S(1)} %convolution_add_fusion.12), channel_id=1, source_target_pairs={{0,4},{4,8},{8,12},{12,16},{16,20},{20,24},{24,28},{1,5},{5,9},{9,... | collective-permute-start | bytes 1572872 | tf_op jit(solution)/shard_map/while/body/eval_jaxpr/ppermute | solution.py:35
  169.8 9.4 %collective-permute-done = f32[8,128,128]{2,1,0:T(8,128)S(1)} collective-permute-done((f32[8,128,128]{2,1,0:T(8,128)S(1)}, f32[8,128,128]{2,1,0:T(8,128)S(1)}, u32[]{:S(2)}, u32[]{:S(2)}) %collective-permute-start) | collective-permute-done | bytes 524320 | tf_op jit(solution)/shard_map/while/body/eval_jaxpr/ppermute | solution.py:35
  179.8 5.3 %collective-permute-start = (f32[8,128,128]{2,1,0:T(8,128)S(1)}, f32[8,128,128]{2,1,0:T(8,128)S(1)}, u32[]{:S(2)}, u32[]{:S(2)}) collective-permute-start(f32[8,128,128]{2,1,0:T(8,128)S(1)} %convolution_add_fusion.12), channel_id=1, source_target_pairs={{0,4},{4,8},{8,12},{12,16},{16,20},{20,24},{24,28},{1,5},{5,9},{9,... | collective-permute-start | bytes 1572872 | tf_op jit(solution)/shard_map/while/body/eval_jaxpr/ppermute | solution.py:35
  185.2 8.6 %collective-permute-done = f32[8,128,128]{2,1,0:T(8,128)S(1)} collective-permute-done((f32[8,128,128]{2,1,0:T(8,128)S(1)}, f32[8,128,128]{2,1,0:T(8,128)S(1)}, u32[]{:S(2)}, u32[]{:S(2)}) %collective-permute-start) | collective-permute-done | bytes 524320 | tf_op jit(solution)/shard_map/while/body/eval_jaxpr/ppermute | solution.py:35
  194.4 5.3 %collective-permute-start = (f32[8,128,128]{2,1,0:T(8,128)S(1)}, f32[8,128,128]{2,1,0:T(8,128)S(1)}, u32[]{:S(2)}, u32[]{:S(2)}) collective-permute-start(f32[8,128,128]{2,1,0:T(8,128)S(1)} %convolution_add_fusion.12), channel_id=1, source_target_pairs={{0,4},{4,8},{8,12},{12,16},{16,20},{20,24},{24,28},{1,5},{5,9},{9,... | collective-permute-start | bytes 1572872 | tf_op jit(solution)/shard_map/while/body/eval_jaxpr/ppermute | solution.py:35
  199.7 7.7 %collective-permute-done = f32[8,128,128]{2,1,0:T(8,128)S(1)} collective-permute-done((f32[8,128,128]{2,1,0:T(8,128)S(1)}, f32[8,128,128]{2,1,0:T(8,128)S(1)}, u32[]{:S(2)}, u32[]{:S(2)}) %collective-permute-start) | collective-permute-done | bytes 524320 | tf_op jit(solution)/shard_map/while/body/eval_jaxpr/ppermute | solution.py:35
  208.1 5.3 %collective-permute-start = (f32[8,128,128]{2,1,0:T(8,128)S(1)}, f32[8,128,128]{2,1,0:T(8,128)S(1)}, u32[]{:S(2)}, u32[]{:S(2)}) collective-permute-start(f32[8,128,128]{2,1,0:T(8,128)S(1)} %convolution_add_fusion.12), channel_id=1, source_target_pairs={{0,4},{4,8},{8,12},{12,16},{16,20},{20,24},{24,28},{1,5},{5,9},{9,... | collective-permute-start | bytes 1572872 | tf_op jit(solution)/shard_map/while/body/eval_jaxpr/ppermute | solution.py:35
  213.4 6.9 %collective-permute-done = f32[8,128,128]{2,1,0:T(8,128)S(1)} collective-permute-done((f32[8,128,128]{2,1,0:T(8,128)S(1)}, f32[8,128,128]{2,1,0:T(8,128)S(1)}, u32[]{:S(2)}, u32[]{:S(2)}) %collective-permute-start) | collective-permute-done | bytes 524320 | tf_op jit(solution)/shard_map/while/body/eval_jaxpr/ppermute | solution.py:35
  220.2 1.3 fusion.45
  221.6 1.9 fusion.39
  226.7 63.4 %reduce-scatter.2.cloned.1.call-done = bf16[2,4,16,128]{3,2,1,0:T(8,128)(2,1)} async-done(((bf16[2,4,128,128]{3,2,1,0:T(8,128)(2,1)}), bf16[2,4,16,128]{3,2,1,0:T(8,128)(2,1)}) %reduce-scatter.2.cloned.1.call-update) | async-done | bytes 32784 | tf_op jit(solution)/shard_map/reduce_scatter | solution.py:220
  292.0 19.7 %all-reduce = (f32[2,4,128]{2,1,0:T(4,128)S(1)}, f32[2,4,128]{2,1,0:T(4,128)S(1)}) all-reduce(f32[2,4,128]{2,1,0:T(4,128)S(1)} %bitcast.225, f32[2,4,128]{2,1,0:T(4,128)S(1)} %bitcast.226), channel_id=1, replica_groups=mesh['sp'=8,'tp'=4] {'sp'}, use_global_device_ids=true, to_apply=%region_13.14 | all-reduce | flops 2048 | bytes 16384 | tf_op jit(solution)/shard_map/psum | solution.py:226
  (131 shorter events, 43.0 us)
Async XLA Ops:
  7.2 37.5 %copy-start = (bf16[4096,4]{0,1:T(4,128)(2,1)S(1)}, bf16[4096,4]{0,1:T(4,128)(2,1)}, u32[]{:S(2)}) copy-start(bf16[4096,4]{0,1:T(4,128)(2,1)} %param.25) | copy-start | bytes 98308
  7.2 35.2 %copy-start.3 = (bf16[2,192,1024]{2,1,0:T(8,128)(2,1)S(1)}, bf16[2,192,1024]{2,1,0:T(8,128)(2,1)}, u32[]{:S(2)}) copy-start(bf16[2,192,1024]{2,1,0:T(8,128)(2,1)} %param.19) | copy-start | bytes 2359300
  7.2 283.0 %reduce-scatter.2.cloned.1.call-start = ((), (), s32[]{:S(2)}) async-start(), calls=%async_computation.1 | async-start | bytes 294912 | tf_op jit(solution)/shard_map/reduce_scatter | solution.py:220
  7.2 12.3 %collective-permute-start.1 = (bf16[2,192,1024]{2,1,0:T(8,128)(2,1)}, bf16[2,192,1024]{2,1,0:T(8,128)(2,1)S(1)}, u32[]{:S(2)}, u32[]{:S(2)}) collective-permute-start(bf16[2,192,1024]{2,1,0:T(8,128)(2,1)} %param.19), channel_id=1, source_target_pairs={{0,3},{1,0},{2,1},{3,2},{4,7},{5,4},{6,5},{7,6},{8,11},{9,8},{10,9... | collective-permute-start | bytes 2359304 | tf_op jit(solution)/shard_map/ppermute | solution.py:18
  19.5 11.3 %collective-permute-start.2 = (bf16[2,192,1024]{2,1,0:T(8,128)(2,1)S(1)}, bf16[2,192,1024]{2,1,0:T(8,128)(2,1)S(1)}, u32[]{:S(2)}, u32[]{:S(2)}) collective-permute-start(bf16[2,192,1024]{2,1,0:T(8,128)(2,1)S(1)} %collective-permute-done.1), channel_id=1, source_target_pairs={{0,3},{1,0},{2,1},{3,2},{4,7},{5,4},{6,5},{7,6},{8,11},{9,8},{10,9... | collective-permute-start | bytes 2359304 | tf_op jit(solution)/shard_map/ppermute | solution.py:18
  30.9 11.4 %collective-permute-start.3 = (bf16[2,192,1024]{2,1,0:T(8,128)(2,1)S(1)}, bf16[2,192,1024]{2,1,0:T(8,128)(2,1)S(1)}, u32[]{:S(2)}, u32[]{:S(2)}) collective-permute-start(bf16[2,192,1024]{2,1,0:T(8,128)(2,1)S(1)} %collective-permute-done.2), channel_id=1, source_target_pairs={{0,3},{1,0},{2,1},{3,2},{4,7},{5,4},{6,5},{7,6},{8,11},{9,8},{10,9... | collective-permute-start | bytes 2359304 | tf_op jit(solution)/shard_map/ppermute | solution.py:18
  43.0 1.7 copy-start.1
  46.5 5.9 %copy-start.2 = (bf16[2,192,4096]{2,1,0:T(8,128)(2,1)S(1)}, bf16[2,192,4096]{2,1,0:T(8,128)(2,1)}, u32[]{:S(2)}) copy-start(bf16[2,192,4096]{2,1,0:T(8,128)(2,1)} %copy-done.1) | copy-start | bytes 9437188
  46.6 5.9 %copy-start.14 = (bf16[4096,512]{1,0:T(8,128)(2,1)S(1)}, bf16[4096,512]{1,0:T(8,128)(2,1)}, u32[]{:S(2)}) copy-start(bf16[4096,512]{1,0:T(8,128)(2,1)} %param.20) | copy-start | bytes 12582916
  54.3 1.0 copy-start.6
  54.3 1.0 copy-start.12
  69.4 1.5 copy-start.7
  116.1 105.5 %copy-start.4 = (f32[3,8,64,128]{3,2,0,1:T(8,128)S(1)}, f32[3,8,64,128]{3,2,0,1:T(8,128)}, u32[]{:S(2)}) copy-start(f32[3,8,64,128]{3,2,0,1:T(8,128)} %get-tuple-element.90) | copy-start | bytes 2359300
  116.8 15.4 %collective-permute-start = (f32[8,128,128]{2,1,0:T(8,128)S(1)}, f32[8,128,128]{2,1,0:T(8,128)S(1)}, u32[]{:S(2)}, u32[]{:S(2)}) collective-permute-start(f32[8,128,128]{2,1,0:T(8,128)S(1)} %convolution_add_fusion.12), channel_id=1, source_target_pairs={{0,4},{4,8},{8,12},{12,16},{16,20},{20,24},{24,28},{1,5},{5,9},{9,... | collective-permute-start | bytes 1572872 | tf_op jit(solution)/shard_map/while/body/eval_jaxpr/ppermute | solution.py:35
  132.9 15.6 %collective-permute-start = (f32[8,128,128]{2,1,0:T(8,128)S(1)}, f32[8,128,128]{2,1,0:T(8,128)S(1)}, u32[]{:S(2)}, u32[]{:S(2)}) collective-permute-start(f32[8,128,128]{2,1,0:T(8,128)S(1)} %convolution_add_fusion.12), channel_id=1, source_target_pairs={{0,4},{4,8},{8,12},{12,16},{16,20},{20,24},{24,28},{1,5},{5,9},{9,... | collective-permute-start | bytes 1572872 | tf_op jit(solution)/shard_map/while/body/eval_jaxpr/ppermute | solution.py:35
  149.1 14.7 %collective-permute-start = (f32[8,128,128]{2,1,0:T(8,128)S(1)}, f32[8,128,128]{2,1,0:T(8,128)S(1)}, u32[]{:S(2)}, u32[]{:S(2)}) collective-permute-start(f32[8,128,128]{2,1,0:T(8,128)S(1)} %convolution_add_fusion.12), channel_id=1, source_target_pairs={{0,4},{4,8},{8,12},{12,16},{16,20},{20,24},{24,28},{1,5},{5,9},{9,... | collective-permute-start | bytes 1572872 | tf_op jit(solution)/shard_map/while/body/eval_jaxpr/ppermute | solution.py:35
  164.5 14.7 %collective-permute-start = (f32[8,128,128]{2,1,0:T(8,128)S(1)}, f32[8,128,128]{2,1,0:T(8,128)S(1)}, u32[]{:S(2)}, u32[]{:S(2)}) collective-permute-start(f32[8,128,128]{2,1,0:T(8,128)S(1)} %convolution_add_fusion.12), channel_id=1, source_target_pairs={{0,4},{4,8},{8,12},{12,16},{16,20},{20,24},{24,28},{1,5},{5,9},{9,... | collective-permute-start | bytes 1572872 | tf_op jit(solution)/shard_map/while/body/eval_jaxpr/ppermute | solution.py:35
  179.8 13.9 %collective-permute-start = (f32[8,128,128]{2,1,0:T(8,128)S(1)}, f32[8,128,128]{2,1,0:T(8,128)S(1)}, u32[]{:S(2)}, u32[]{:S(2)}) collective-permute-start(f32[8,128,128]{2,1,0:T(8,128)S(1)} %convolution_add_fusion.12), channel_id=1, source_target_pairs={{0,4},{4,8},{8,12},{12,16},{16,20},{20,24},{24,28},{1,5},{5,9},{9,... | collective-permute-start | bytes 1572872 | tf_op jit(solution)/shard_map/while/body/eval_jaxpr/ppermute | solution.py:35
  194.4 13.0 %collective-permute-start = (f32[8,128,128]{2,1,0:T(8,128)S(1)}, f32[8,128,128]{2,1,0:T(8,128)S(1)}, u32[]{:S(2)}, u32[]{:S(2)}) collective-permute-start(f32[8,128,128]{2,1,0:T(8,128)S(1)} %convolution_add_fusion.12), channel_id=1, source_target_pairs={{0,4},{4,8},{8,12},{12,16},{16,20},{20,24},{24,28},{1,5},{5,9},{9,... | collective-permute-start | bytes 1572872 | tf_op jit(solution)/shard_map/while/body/eval_jaxpr/ppermute | solution.py:35
  208.1 12.2 %collective-permute-start = (f32[8,128,128]{2,1,0:T(8,128)S(1)}, f32[8,128,128]{2,1,0:T(8,128)S(1)}, u32[]{:S(2)}, u32[]{:S(2)}) collective-permute-start(f32[8,128,128]{2,1,0:T(8,128)S(1)} %convolution_add_fusion.12), channel_id=1, source_target_pairs={{0,4},{4,8},{8,12},{12,16},{16,20},{20,24},{24,28},{1,5},{5,9},{9,... | collective-permute-start | bytes 1572872 | tf_op jit(solution)/shard_map/while/body/eval_jaxpr/ppermute | solution.py:35
  223.6 2.2 copy-start.5
  223.9 66.3 %copy-start.10 = (f32[2,4,16]{2,1,0:T(4,128)S(1)}, f32[2,4,16]{2,1,0:T(4,128)}, u32[]{:S(2)}) copy-start(f32[2,4,16]{2,1,0:T(4,128)} %get-tuple-element.259) | copy-start | bytes 1540
  223.9 67.2 %copy-start.9 = (f32[2,4,16]{2,1,0:T(4,128)S(1)}, f32[2,4,16]{2,1,0:T(4,128)}, u32[]{:S(2)}) copy-start(f32[2,4,16]{2,1,0:T(4,128)} %get-tuple-element.260) | copy-start | bytes 1540
  223.9 87.8 %copy-start.8 = (bf16[2,4,128]{2,1,0:T(4,128)(2,1)S(1)}, bf16[2,4,128]{2,1,0:T(4,128)(2,1)}, u32[]{:S(2)}) copy-start(bf16[2,4,128]{2,1,0:T(4,128)(2,1)} %param.31) | copy-start | bytes 6148
  223.9 87.8 %copy-start.11 = (f32[2,4]{1,0:T(2,128)S(1)}, f32[2,4]{1,0:T(2,128)}, u32[]{:S(2)}) copy-start(f32[2,4]{1,0:T(2,128)} %param.33) | copy-start | bytes 100
  223.9 88.0 %copy-start.13 = (f32[128]{0:T(128)S(1)}, f32[128]{0:T(128)}, u32[]{:S(2)}) copy-start(f32[128]{0:T(128)} %param.28) | copy-start | bytes 1540
Sparse Core Ops, SparseCore 0:
  221.7 68.3 reduce-scatter.1
